TPU v7x, 32 devices: a whole 2x2x4 slice. The times are simulated.
32 devices in a mesh: sp: 8 (over z, y), tp: 4 (over x, core).
Axes of the slice: x: 2, y: 2, z: 4, core: 2. Of those that a mesh axis runs over, the one named last changes fastest.
Arguments:
- residual_in: bfloat16 [16384, 2048], P(('sp', 'tp')), may hold values from -6 to 6
- conv_input: bfloat16 [16384, 1024], P('sp', 'tp'), may hold values from -6 to 6
- input_gate: bfloat16 [16384, 1024], P('sp', 'tp'), may hold values from -6 to 6
- output_gate: bfloat16 [16384, 1024], P('sp', 'tp'), may hold values from -6 to 6
- conv_taps: bfloat16 [3, 1024], P(None, 'tp'), may hold values from -3.5 to 3.5
- doc_ids: int32 [16384], P('sp'), may hold values from 0 to 3, never falling along the last dimension, each value on 1 to 8192 neighbouring positions
- proj_weight: bfloat16 [1024, 2048], replicated, may hold values from -0.1875 to 0.1875
- norm_gain: float32 [2048], replicated, may hold values from 0.1 to 1.9
- expert_ids: int32 [16384, 2], P(('sp', 'tp')), may hold values from 0 to 31, all different within a row; in each aligned block of 512 rows (0 to 511, 512 to 1023, ...) at most 64 rows name the same one
- expert_weight: float32 [16384, 2], P(('sp', 'tp')), may hold values from 0.05 to 1
- w_gate: bfloat16 [32, 2048, 512], P('sp'), may hold values from -0.125 to 0.125
- w_up: bfloat16 [32, 2048, 512], P('sp'), may hold values from -0.125 to 0.125
- w_down: bfloat16 [32, 512, 2048], P('sp'), may hold values from -0.25 to 0.25
Outputs:
- layer_out: bfloat16 [16384, 2048], P(('sp', 'tp'))
Inputs may be any that keep to these rules, and one draw needn't show every extreme that they name: `doc_ids`: numbers never fall along the sequence; one document spans at most 8192 positions. `expert_ids`: a token's two experts differ; in each aligned block of rows that one device holds, no expert is named more than 64 times, a bound that some block reaches.
All inputs are finite; a program needn't handle non-finite values.
Results may differ from a plain program's by a relative error of at most 0.0047.
Values may be sent and summed in bfloat16 or wider, within the bound.
A program may use at most 128 MiB of HBM per device.

v0:
```python
import functools

import jax
import jax.numpy as jnp
from jax import lax
from jax.experimental import pallas as pl
from jax.experimental.pallas import tpu as pltpu
from jax.sharding import PartitionSpec as P

CAP = 64
PLANES = 4
CHUNKS = 4
BLOCK = 128
HALF = 256
epsilon = 1e-06
MESH = pl.DeviceIdType.MESH
bf16, f32 = jnp.bfloat16, jnp.float32


def lookup(table, p, k):
    out = 0
    for i, row in enumerate(table):
        for j, v in enumerate(row):
            out = out + jnp.where((p == i) & (k == j), v, 0)
    return out


ORDER = ((0, 1, 2, 3), (1, 0, 2, 3), (2, 3, 1, 0), (3, 2, 1, 0))
LOW = ((0, 1, 2, 3), (0, 1, 3, 3), (0, 1, 3, 3), (0, 1, 2, 3))
HIGH = ((1, 2, 3, 4), (1, 3, 3, 4), (1, 3, 3, 4), (1, 2, 3, 4))


def moe_kernel(
    rest,
    normed_hbm,
    meta_hbm,
    hidden_hbm,
    gate_hbm,
    up_hbm,
    down_hbm,
    out_hbm,
    tok,
    meta,
    slots,
    away,
    back,
    parts,
    gate,
    up,
    down,
    pick,
    mix,
    hid,
    fin,
    load_sem,
    meta_load_sem,
    weight_sem,
    own_sem,
    own_meta_sem,
    tok_send,
    tok_recv,
    meta_send,
    meta_recv,
    away_send,
    away_recv,
    back_send,
    back_recv,
    part_send,
    part_recv,
    hid_sem,
    fin_sem,
):
    me = lax.axis_index("sp")
    p, r = me // rest, lax.rem(me, rest)
    first, last = p == 0, p == PLANES - 1
    inner = jnp.logical_not(first | last)
    below = lax.max(me - rest, 0)
    above = lax.min(me + rest, PLANES * rest - 1)
    experts, _, hidden_width = gate.shape
    tokens, width = tok.shape[2], tok.shape[3]
    local = experts * CAP
    peers = [p * rest + lax.rem(r + d, rest) for d in range(1, rest)]
    origins = [p * rest + lax.rem(r + rest - d, rest) for d in range(1, rest)]

    def remote(src, dst, send, recv, device):
        return pltpu.make_async_remote_copy(
            src_ref=src, dst_ref=dst, send_sem=send, recv_sem=recv, device_id={"sp": device}, device_id_type=MESH
        )

    def token_copy(s, c, send, device):
        return remote(tok.at[s, c], tok.at[s, c], send, tok_recv.at[s, c], device)

    def meta_copy(s, send, device):
        return remote(meta.at[s], meta.at[s], send, meta_recv.at[s], device)

    def away_copy(s, d, c):
        peer = peers[d]
        return remote(slots.at[s, lax.rem(r + d + 1, rest), c], away.at[s, d, c], away_send.at[s, d, c], away_recv.at[s, d, c], peer)

    def back_copy(s, d, e):
        return remote(away.at[s, d, :, e], back.at[s, d, :, e], back_send.at[s, d, e], back_recv.at[s, d, e], origins[d])

    def part_copy(s, c):
        down_way = p > s
        target = jnp.where(down_way, below, above)
        index = jnp.where(down_way & (p - 1 == s), PLANES, s)
        return remote(tok.at[s, c], parts.at[index, c], part_send.at[s, c], part_recv.at[index, c], target)

    def part_arrival(index, c):
        return remote(tok.at[0, c], parts.at[index, c], part_send.at[0, c], part_recv.at[index, c], below)

    loads = [
        pltpu.make_async_copy(normed_hbm.at[:, pl.ds(c * width, width)], tok.at[p, c], load_sem.at[c]) for c in range(CHUNKS)
    ]
    meta_load = pltpu.make_async_copy(meta_hbm, meta.at[p], meta_load_sem)

    def weight_copies(e):
        pairs = ((gate_hbm, gate), (up_hbm, up), (down_hbm, down))
        return [pltpu.make_async_copy(a.at[e], b.at[e], weight_sem.at[i, e]) for i, (a, b) in enumerate(pairs)]

    meta_load.start()
    for load in loads:
        load.start()
    barrier = pltpu.get_barrier_semaphore()

    @pl.when(jnp.logical_not(first))
    def _():
        pl.semaphore_signal(barrier, inc=1, device_id={"sp": below}, device_id_type=MESH)

    @pl.when(jnp.logical_not(last))
    def _():
        pl.semaphore_signal(barrier, inc=1, device_id={"sp": above}, device_id_type=MESH)

    for peer in peers:
        pl.semaphore_signal(barrier, inc=1, device_id={"sp": peer}, device_id_type=MESH)
    pl.semaphore_wait(barrier, rest - 1 + jnp.where(inner, 2, 1))

    def own_copy(way, c):
        device = (above, below)[way]
        if c == 0:
            return meta_copy(p, own_meta_sem.at[way], device)
        return token_copy(p, c - 1, own_sem.at[way, c - 1], device)

    ways = (jnp.logical_not(last), jnp.logical_not(first))
    meta_load.wait()
    for c in range(CHUNKS + 1):
        if c:
            loads[c - 1].wait()
        for way in range(2):

            @pl.when(ways[way])
            def _():
                own_copy(way, c).start()

    for e in range(experts):
        for copy in weight_copies(e):
            copy.start()

    def unpack_step(k, carry):
        s = lookup(ORDER, p, k)
        onward = jnp.where(s < p, above, below)
        fresh = k > 0

        @pl.when(fresh)
        def _():
            meta_copy(s, meta_send.at[s], onward).wait_recv()

        @pl.when(fresh & inner)
        def _():
            meta_copy(s, meta_send.at[s], onward).start()

        def pick_rows(q, carry):
            base = (p * rest * local + q * BLOCK).astype(f32)
            names = lax.broadcasted_iota(jnp.int32, (BLOCK, tokens), 0).astype(f32)
            hit = (names == meta[s, 0:1] - base) | (names == meta[s, 1:2] - base)
            pick[pl.ds(pl.multiple_of(q * BLOCK, BLOCK), BLOCK), :] = jnp.where(hit, 1.0, 0.0).astype(bf16)
            return carry

        lax.fori_loop(0, rest * local // BLOCK, pick_rows, 0)

        def chunk(c, carry):
            @pl.when(fresh)
            def _():
                token_copy(s, c, tok_send.at[s, c], onward).wait_recv()

            @pl.when(fresh & inner)
            def _():
                token_copy(s, c, tok_send.at[s, c], onward).start()

            def pack(q, carry):
                chosen = pick[pl.ds(pl.multiple_of(q * local, local), local), :]
                rows = jnp.dot(chosen, tok[s, c], preferred_element_type=f32).astype(bf16)
                slots[s, q, c] = rows.reshape(experts, CAP, width)
                return carry

            lax.fori_loop(0, rest, pack, 0)
            for d in range(rest - 1):
                away_copy(s, d, c).start()
            return carry

        return lax.fori_loop(0, CHUNKS, chunk, carry)

    def expert_step(k):
        s = lookup(ORDER, p, k)
        for d in range(rest - 1):
            for c in range(CHUNKS):
                away_copy(s, d, c).wait_recv()

        def one(e, carry):
            @pl.when(k == 0)
            def _():
                for copy in weight_copies(e):
                    copy.wait()

            gate_val = jnp.zeros((rest * CAP, hidden_width), f32)
            up_val = jnp.zeros((rest * CAP, hidden_width), f32)
            for c in range(CHUNKS):
                x = jnp.concatenate([slots[s, r, c, e]] + [away[s, d, c, e] for d in range(rest - 1)], axis=0)
                rows = pl.ds(c * width, width)
                gate_val = gate_val + jnp.dot(x, gate[e, rows, :], preferred_element_type=f32)
                up_val = up_val + jnp.dot(x, up[e, rows, :], preferred_element_type=f32)
            act = (gate_val * jax.nn.sigmoid(gate_val) * up_val).astype(bf16)
            for c in range(CHUNKS):
                out = jnp.dot(act, down[e, :, pl.ds(c * width, width)], preferred_element_type=f32).astype(bf16)
                slots[s, r, c, e] = out[:CAP]
                for d in range(rest - 1):
                    away[s, d, c, e] = out[(d + 1) * CAP : (d + 2) * CAP]
            for d in range(rest - 1):
                back_copy(s, d, e).start()
            return carry

        lax.fori_loop(0, experts, one, 0)

    def make_mix(s, i):
        def rows(q, carry):
            here = pl.ds(pl.multiple_of(q * BLOCK, BLOCK), BLOCK)
            info = meta[s, :, here].T
            names = lax.broadcasted_iota(jnp.int32, (BLOCK, local), 1).astype(f32)
            for d in range(rest):
                base = (p * rest * local + lax.rem(r + d, rest) * local).astype(f32)
                mix[i, d, here] = (
                    jnp.where(names == info[:, 0:1] - base, info[:, 2:3], 0.0)
                    + jnp.where(names == info[:, 1:2] - base, info[:, 3:4], 0.0)
                ).astype(bf16)
            return carry

        lax.fori_loop(0, tokens // BLOCK, rows, 0)

    def returns(s):
        for d in range(rest - 1):
            for e in range(experts):
                back_copy(s, d, e).wait_recv()

    def combine(s, i, c, here):
        acc = jnp.dot(mix[i, 0, here], slots[s, r, c].reshape(local, width), preferred_element_type=f32)
        for d in range(rest - 1):
            acc = acc + jnp.dot(mix[i, d + 1, here], back[s, d, c].reshape(local, width), preferred_element_type=f32)
        return acc

    def by_rows(step):
        def body(q, carry):
            step(pl.ds(pl.multiple_of(q * HALF, HALF), HALF))
            return carry

        lax.fori_loop(0, tokens // HALF, body, 0)

    def send_part(s, i, c, passed):
        if passed:
            part_arrival(s, c).wait_recv()
            token_copy(s, c, tok_send.at[s, c], below).wait_send()

        def step(here):
            acc = combine(s, i, c, here)
            if passed:
                acc = acc + parts[s, c, here].astype(f32)
            tok[s, c, here] = acc.astype(bf16)

        by_rows(step)
        part_copy(s, c).start()

    def main_step(k, carry):
        lax.fori_loop(lookup(LOW, p, k), lookup(HIGH, p, k), unpack_step, 0)
        expert_step(k)

        @pl.when((k > 0) & jnp.logical_not(inner))
        def _():
            s = lookup(ORDER, p, k)
            returns(s)
            make_mix(s, 0)

            def chunk(c, carry):
                send_part(s, 0, c, False)
                return carry

            lax.fori_loop(0, CHUNKS, chunk, 0)

        return carry

    lax.fori_loop(0, PLANES, main_step, 0)

    @pl.when(inner)
    def _():
        near = PLANES - 1 - p
        end = jnp.where(p == 1, PLANES - 1, 0)
        far = PLANES - 1 - end
        returns(near)
        make_mix(near, 0)

        def one(c, carry):
            send_part(near, 0, c, True)
            return carry

        lax.fori_loop(0, CHUNKS, one, 0)
        returns(end)
        returns(far)
        make_mix(end, 0)
        make_mix(far, 1)

        def two(c, carry):
            send_part(end, 0, c, True)
            send_part(far, 1, c, True)
            return carry

        lax.fori_loop(0, CHUNKS, two, 0)

    def fin_copy(c):
        return pltpu.make_async_copy(fin.at[c % 2], out_hbm.at[:, pl.ds(c * width, width)], fin_sem.at[c % 2])

    returns(p)
    make_mix(p, 0)
    for c in range(CHUNKS):
        hid_copy = pltpu.make_async_copy(hidden_hbm.at[:, pl.ds(c * width, width)], hid, hid_sem)
        hid_copy.start()
        hid_copy.wait()

        @pl.when(jnp.logical_not(first))
        def _():
            part_arrival(p, c).wait_recv()

            def step(here):
                hid[here] = hid[here] + parts[p, c, here].astype(f32)

            by_rows(step)

        @pl.when(jnp.logical_not(last))
        def _():
            part_arrival(PLANES, c).wait_recv()

            def step(here):
                hid[here] = hid[here] + parts[PLANES, c, here].astype(f32)

            by_rows(step)

        def step(here):
            fin[c % 2, here] = (hid[here] + combine(p, 0, c, here)).astype(bf16)

        by_rows(step)
        fin_copy(c).start()
        if c:
            fin_copy(c - 1).wait()
    fin_copy(CHUNKS - 1).wait()

    for way in range(2):

        @pl.when(ways[way])
        def _():
            for c in range(CHUNKS + 1):
                own_copy(way, c).wait_send()

    def drain(k, carry):
        s = lookup(ORDER, p, k)
        for d in range(rest - 1):
            for c in range(CHUNKS):
                away_copy(s, d, c).wait_send()
            for e in range(experts):
                back_copy(s, d, e).wait_send()

        @pl.when(k > 0)
        def _():
            for c in range(CHUNKS):
                part_copy(s, c).wait_send()

        @pl.when((k > 0) & inner)
        def _():
            meta_copy(s, meta_send.at[s], below).wait_send()

        return carry

    lax.fori_loop(0, PLANES, drain, 0)


def experts_and_back(normed, meta, hidden, w_gate, w_up, w_down):
    rest = lax.axis_size("sp") // PLANES
    experts, model, ffe = w_gate.shape
    tokens = normed.shape[0]
    width = model // CHUNKS
    dma = pltpu.SemaphoreType.DMA
    anywhere = pl.BlockSpec(memory_space=pl.ANY)
    return pl.pallas_call(
        functools.partial(moe_kernel, rest),
        in_specs=[anywhere] * 6,
        out_specs=anywhere,
        out_shape=jax.ShapeDtypeStruct((tokens, model), bf16),
        scratch_shapes=[
            pltpu.VMEM((PLANES, CHUNKS, tokens, width), bf16),
            pltpu.VMEM((PLANES,) + meta.shape, f32),
            pltpu.VMEM((PLANES, rest, CHUNKS, experts, CAP, width), bf16),
            pltpu.VMEM((PLANES, rest - 1, CHUNKS, experts, CAP, width), bf16),
            pltpu.VMEM((PLANES, rest - 1, CHUNKS, experts, CAP, width), bf16),
            pltpu.VMEM((PLANES + 1, CHUNKS, tokens, width), bf16),
            pltpu.VMEM(w_gate.shape, bf16),
            pltpu.VMEM(w_up.shape, bf16),
            pltpu.VMEM(w_down.shape, bf16),
            pltpu.VMEM((rest * experts * CAP, tokens), bf16),
            pltpu.VMEM((2, rest, tokens, experts * CAP), bf16),
            pltpu.VMEM((tokens, width), f32),
            pltpu.VMEM((2, tokens, width), bf16),
            dma((CHUNKS,)),
            dma,
            dma((3, experts)),
            dma((2, CHUNKS)),
            dma((2,)),
            dma((PLANES, CHUNKS)),
            dma((PLANES, CHUNKS)),
            dma((PLANES,)),
            dma((PLANES,)),
            dma((PLANES, rest - 1, CHUNKS)),
            dma((PLANES, rest - 1, CHUNKS)),
            dma((PLANES, rest - 1, experts)),
            dma((PLANES, rest - 1, experts)),
            dma((PLANES, CHUNKS)),
            dma((PLANES + 1, CHUNKS)),
            dma,
            dma((2,)),
        ],
        compiler_params=pltpu.CompilerParams(collective_id=0, has_side_effects=True, vmem_limit_bytes=67043328),
        cost_estimate=pl.CostEstimate(
            flops=6 * PLANES * rest * experts * CAP * model * ffe,
            bytes_accessed=2 * (w_gate.size * 3 + 4 * normed.size),
            transcendentals=PLANES * rest * experts * CAP * ffe,
        ),
    )(normed, meta, hidden, w_gate, w_up, w_down)


def from_behind(x, axis, by):
    devices = lax.axis_size(axis)
    pairs = [(i, i + by) for i in range(devices) if 0 <= i + by < devices]
    return lax.ppermute(x, axis, pairs)


def slot_table(ids, weights, experts):
    tokens = ids.shape[1]
    names = jnp.arange(experts, dtype=jnp.int32)[:, None]
    hits = [ids[j][None, :] == names for j in range(2)]
    named = (hits[0] | hits[1]).astype(bf16)
    at = jnp.arange(tokens, dtype=jnp.int32)
    earlier = (at[:, None] < at[None, :]).astype(bf16)
    before = jnp.dot(named, earlier, preferred_element_type=f32)
    rank = [jnp.sum(jnp.where(hits[j], before, 0.0), axis=0) for j in range(2)]
    slot = [ids[j].astype(f32) * CAP + rank[j] for j in range(2)]
    return jnp.concatenate([jnp.stack(slot), weights, jnp.zeros((4, tokens), f32)], axis=0)


def per_device(
    residual_in,
    conv_input,
    input_gate,
    output_gate,
    conv_taps,
    doc_ids,
    proj_weight,
    norm_gain,
    expert_ids,
    expert_weight,
    w_gate,
    w_up,
    w_down,
):
    kernel_width = conv_taps.shape[0]
    rim_rows = kernel_width - 1
    meta = slot_table(expert_ids.T, expert_weight.T, w_gate.shape[0] * lax.axis_size("sp"))

    product = input_gate.astype(f32) * conv_input.astype(f32)
    doc_float = doc_ids.astype(f32)
    doc_rim = jnp.broadcast_to(doc_float[-rim_rows:, None], (rim_rows, 128))
    rim = from_behind(jnp.concatenate([product[-rim_rows:], doc_rim], axis=1), "sp", 1)
    channels = product.shape[1]
    prev_in, prev_ids = rim[:, :channels], rim[:, channels]
    prev_ids = jnp.where(lax.axis_index("sp") == 0, -1.0, prev_ids)
    padded_in = jnp.concatenate([prev_in, product], axis=0)
    padded_ids = jnp.concatenate([prev_ids, doc_float], axis=0)
    length = product.shape[0]
    conv_sum = jnp.zeros(product.shape, f32)
    for offset in range(kernel_width):
        same_doc = padded_ids[offset : offset + length] == doc_float
        term = conv_taps[offset].astype(f32)[None, :] * padded_in[offset : offset + length]
        conv_sum = conv_sum + jnp.where(same_doc[:, None], term, 0.0)
    gated = (output_gate.astype(f32) * conv_sum).astype(bf16)
    regrouped = lax.all_to_all(gated, "tp", split_axis=0, concat_axis=1, tiled=True)

    mixed = jnp.dot(regrouped, proj_weight, preferred_element_type=f32)
    hidden = residual_in.astype(f32) + mixed
    scale_rows = lax.rsqrt(jnp.mean(hidden * hidden, axis=-1, keepdims=True) + epsilon)
    normed = (hidden * scale_rows * norm_gain[None, :]).astype(bf16)
    return experts_and_back(normed, meta, hidden, w_gate, w_up, w_down)


def solution(mesh):
    return jax.shard_map(
        per_device,
        mesh=mesh,
        in_specs=(
            P(("sp", "tp"), None),
            P("sp", "tp"),
            P("sp", "tp"),
            P("sp", "tp"),
            P(None, "tp"),
            P("sp"),
            P(),
            P(),
            P(("sp", "tp"), None),
            P(("sp", "tp"), None),
            P("sp", None, None),
            P("sp", None, None),
            P("sp", None, None),
        ),
        out_specs=P(("sp", "tp"), None),
        check_vma=False,
    )
```

profile of v0, /device:TPU:16, one launch (start us, length us, event | category | flops | bytes accessed | tf_op | source)
XLA Modules:
  0.0 316.2 jit_solution(8248271059041104087)
XLA Ops:
  0.0 0.7 convert_element_type.41
  0.7 0.1 slice.55
  0.8 1.9 convert_multiply_fusion
  2.7 0.1 broadcast_in_dim.54
  2.7 3.4 %collective-permute-start = (f32[2,384]{1,0:T(2,128)S(1)}, f32[2,384]{1,0:T(2,128)S(1)}, u32[]{:S(2)}, u32[]{:S(2)}) collective-permute-start(f32[2,384]{1,0:T(2,128)S(1)} %pad_maximum_fusion.2), channel_id=1, source_target_pairs={{0,4},{4,8},{8,12},{12,16},{16,20},{20,24},{24,28},{1,5},{5,9},{9,... | collective-permute-start | bytes 9224 | tf_op jit(solution)/shard_map/ppermute | solution.py:448
  6.2 0.0 copy-done.2
  6.2 0.0 copy-done.5
  6.2 0.1 pad.3.clone
  6.3 2.8 collective-permute-done
  9.1 0.1 fusion.17
  9.2 0.1 fusion.15
  9.3 0.0 copy-done.1
  9.3 3.3 %fusion.6 = bf16[2048,256]{1,0:T(8,128)(2,1)} fusion(f32[2,256]{1,0:T(2,128)S(1)} %slice.59, f32[2048,256]{1,0:T(8,128)S(1)} %convert_multiply_fusion, bf16[2048,256]{1,0:T(8,128)(2,1)S(1)} %copy-done.1, f32[256]{0:T(256)S(1)} %bitcast.19, f32[256]{0:T(256)S(1)} %bitcast.20, f32[256]{0:T(256)S(1)} %bitcast.18, pred[2048]{0:T(1024)(128)(4,1)S(1)} %convert_compare_fusion, ...), kind=kLoop, calls=%fused_computation.11 | loop fusion | flops 6815744 | bytes 4205568 | tf_op jit(solution)/shard_map/convert_element_type | solution.py:498
  12.7 3.6 %all-to-all-start = ((bf16[4,512,256]{2,1,0:T(8,128)(2,1)}), bf16[4,512,256]{2,1,0:T(8,128)(2,1)S(1)}, u32[]{:S(2)}, u32[]{:S(2)}) async-start(bf16[4,512,256]{2,1,0:T(8,128)(2,1)} %bitcast.3), calls=%async_computation | async-start | bytes 2097152 | tf_op jit(solution)/shard_map/all_to_all | solution.py:499
  16.4 0.2 select_reduce_fusion.1
  16.6 0.7 maximum_maximum_fusion.meta_hbm
  17.3 13.5 %all-to-all-done = bf16[4,512,256]{2,1,0:T(8,128)(2,1)S(1)} async-done(((bf16[4,512,256]{2,1,0:T(8,128)(2,1)}), bf16[4,512,256]{2,1,0:T(8,128)(2,1)S(1)}, u32[]{:S(2)}, u32[]{:S(2)}) %all-to-all-start) | async-done | bytes 1048608 | tf_op jit(solution)/shard_map/all_to_all | solution.py:499
  30.7 0.5 copy.15
  31.3 0.0 copy-start.4
  31.3 5.5 %multiply_reduce_fusion = (f32[512]{0:T(512)S(1)}, f32[512,2048]{1,0:T(8,128)S(1)}) fusion(bf16[512,1024]{0,1:T(8,128)(2,1)S(1)} %bitcast.14, bf16[1024,2048]{1,0:T(8,128)(2,1)} %param.19, bf16[512,2048]{1,0:T(8,128)(2,1)} %param.13), kind=kOutput, calls=%fused_computation.1 | convolution fusion | flops 2151677440 | bytes 11536384 | tf_op jit(solution)/shard_map/dot_general | solution.py:501
  36.8 1.9 copy-done
  38.8 1.7 multiply_convert_fusion.normed_hbm
  40.5 272.5 %shard_map.127 = bf16[512,2048]{1,0:T(8,128)(2,1)} custom-call(bf16[512,2048]{1,0:T(8,128)(2,1)} %multiply_convert_fusion.normed_hbm, f32[8,512]{1,0:T(8,128)} %maximum_maximum_fusion.meta_hbm, f32[512,2048]{1,0:T(8,128)} %copy-done, bf16[4,2048,512]{2,1,0:T(8,128)(2,1)} %gate_hbm.1, bf16[4,2048,512]{2,1,0:T(8,128)(2,1)} %up_hbm.1, ...), custom_call_target="tpu_custom_call" | custom-call | flops 12884901888 | bytes 33554432 | tf_op jit(solution)/shard_map/pallas_call | solution.py:399
  313.0 3.2 copy.17
  (18 shorter events, 0.1 us)
Async XLA Ops:
  0.8 5.4 %copy-start.2 = (s32[2048]{0:T(1024)S(1)}, s32[2048]{0:T(1024)}, u32[]{:S(2)}) copy-start(s32[2048]{0:T(1024)} %param.18) | copy-start | bytes 24580
  0.8 5.4 %copy-start.5 = (bf16[3,256]{1,0:T(4,128)(2,1)S(1)}, bf16[3,256]{1,0:T(4,128)(2,1)}, u32[]{:S(2)}) copy-start(bf16[3,256]{1,0:T(4,128)(2,1)} %param.17) | copy-start | bytes 4612
  0.8 8.5 %copy-start.1 = (bf16[2048,256]{1,0:T(8,128)(2,1)S(1)}, bf16[2048,256]{1,0:T(8,128)(2,1)}, u32[]{:S(2)}) copy-start(bf16[2048,256]{1,0:T(8,128)(2,1)} %param.16) | copy-start | bytes 3145732
  2.7 6.4 %collective-permute-start = (f32[2,384]{1,0:T(2,128)S(1)}, f32[2,384]{1,0:T(2,128)S(1)}, u32[]{:S(2)}, u32[]{:S(2)}) collective-permute-start(f32[2,384]{1,0:T(2,128)S(1)} %pad_maximum_fusion.2), channel_id=1, source_target_pairs={{0,4},{4,8},{8,12},{12,16},{16,20},{20,24},{24,28},{1,5},{5,9},{9,... | collective-permute-start | bytes 9224 | tf_op jit(solution)/shard_map/ppermute | solution.py:448
  12.7 3.7 %copy-start.3 = (s32[512,2]{0,1:T(2,128)S(1)}, s32[512,2]{0,1:T(2,128)}, u32[]{:S(2)}) copy-start(s32[512,2]{0,1:T(2,128)} %param.21) | copy-start | bytes 12292
  12.7 3.9 %copy-start.6 = (f32[512,2]{0,1:T(2,128)S(1)}, f32[512,2]{0,1:T(2,128)}, u32[]{:S(2)}) copy-start(f32[512,2]{0,1:T(2,128)} %param.22) | copy-start | bytes 12292
  12.7 18.1 %all-to-all-start = ((bf16[4,512,256]{2,1,0:T(8,128)(2,1)}), bf16[4,512,256]{2,1,0:T(8,128)(2,1)S(1)}, u32[]{:S(2)}, u32[]{:S(2)}) async-start(bf16[4,512,256]{2,1,0:T(8,128)(2,1)} %bitcast.3), calls=%async_computation | async-start | bytes 2097152 | tf_op jit(solution)/shard_map/all_to_all | solution.py:499
  31.3 7.5 %copy-start.4 = (f32[2048]{0:T(1024)S(1)}, f32[2048]{0:T(1024)}, u32[]{:S(2)}) copy-start(f32[2048]{0:T(1024)} %param.20) | copy-start | bytes 24580
  36.8 1.9 copy-start
where the time goes:
time: 320 us; the launch traced here: 316 us
  Pallas kernels  272 us (85%)
  waiting for transfers between devices  16.3 us (5%)
  other arithmetic  8.53 us (3%)
  starting transfers between devices  7.07 us (2%)
  local copies, waits for them, and re-layouts  5.87 us (2%)
  matrix products  5.75 us (2%)
    pallas_call x1, Pallas kernels, experts_and_back(): pl.pallas_call(functools.partial(moe_kernel, rest), in_specs=[anywhere] *...  272 us
    all_to_all x1, waiting for transfers between devices, per_device(): lax.all_to_all(gated, 'tp', split_axis=0, concat_axis=1, tiled=True)  13.5 us
  transfers between devices with their start and end apart: 2, of which 2 were waited for; matrix products, arithmetic and copies ran while one was open for 0% of the time, Pallas kernels for 0%

commit v1 on v0

--- a/solution.py
+++ b/solution.py
@@ -25,9 +25,9 @@
     return out
 
 
-ORDER = ((0, 1, 2, 3), (1, 0, 2, 3), (2, 3, 1, 0), (3, 2, 1, 0))
+ORDER = ((0, 1, 3, 2), (1, 0, 3, 2), (2, 3, 0, 1), (3, 2, 0, 1))
 LOW = ((0, 1, 2, 3), (0, 1, 3, 3), (0, 1, 3, 3), (0, 1, 2, 3))
-HIGH = ((1, 2, 3, 4), (1, 3, 3, 4), (1, 3, 3, 4), (1, 2, 3, 4))
+HIGH = ((1, 2, 2, 3), (1, 3, 3, 4), (1, 3, 3, 4), (1, 2, 2, 3))
 
 
 def moe_kernel(
@@ -50,6 +50,7 @@
     down,
     pick,
     mix,
+    act,
     hid,
     fin,
     load_sem,
@@ -97,8 +98,8 @@
         peer = peers[d]
         return remote(slots.at[s, lax.rem(r + d + 1, rest), c], away.at[s, d, c], away_send.at[s, d, c], away_recv.at[s, d, c], peer)
 
-    def back_copy(s, d, e):
-        return remote(away.at[s, d, :, e], back.at[s, d, :, e], back_send.at[s, d, e], back_recv.at[s, d, e], origins[d])
+    def back_copy(s, d, c):
+        return remote(away.at[s, d, c], back.at[s, d, c], back_send.at[s, d, c], back_recv.at[s, d, c], origins[d])
 
     def part_copy(s, c):
         down_way = p > s
@@ -142,13 +143,14 @@
         return token_copy(p, c - 1, own_sem.at[way, c - 1], device)
 
     ways = (jnp.logical_not(last), jnp.logical_not(first))
+    middle = (p == 1, p == PLANES - 2)
     meta_load.wait()
     for c in range(CHUNKS + 1):
         if c:
             loads[c - 1].wait()
         for way in range(2):
 
-            @pl.when(ways[way])
+            @pl.when(ways[way] if c < 2 else ways[way] & jnp.logical_not(middle[way]))
             def _():
                 own_copy(way, c).start()
 
@@ -156,7 +158,7 @@
         for copy in weight_copies(e):
             copy.start()
 
-    def unpack_step(k, carry):
+    def unpack_start(k):
         s = lookup(ORDER, p, k)
         onward = jnp.where(s < p, above, below)
         fresh = k > 0
@@ -178,27 +180,45 @@
 
         lax.fori_loop(0, rest * local // BLOCK, pick_rows, 0)
 
+    def unpack_chunk(k, c):
+        s = lookup(ORDER, p, k)
+        onward = jnp.where(s < p, above, below)
+        fresh = k > 0
+
+        @pl.when(fresh)
+        def _():
+            token_copy(s, c, tok_send.at[s, c], onward).wait_recv()
+
+        @pl.when(fresh & inner)
+        def _():
+            token_copy(s, c, tok_send.at[s, c], onward).start()
+
+        def pack(q, carry):
+            chosen = pick[pl.ds(pl.multiple_of(q * local, local), local), :]
+            rows = jnp.dot(chosen, tok[s, c], preferred_element_type=f32).astype(bf16)
+            slots[s, q, c] = rows.reshape(experts, CAP, width)
+            return carry
+
+        lax.fori_loop(0, rest, pack, 0)
+        for d in range(rest - 1):
+            away_copy(s, d, c).start()
+
+    def unpack_step(k, carry):
+        unpack_start(k)
+
         def chunk(c, carry):
-            @pl.when(fresh)
+            unpack_chunk(k, c)
+            return carry
+
+        lax.fori_loop(0, CHUNKS, chunk, 0)
+        for way in range(2):
+
+            @pl.when(middle[way] & (k == 1))
             def _():
-                token_copy(s, c, tok_send.at[s, c], onward).wait_recv()
-
-            @pl.when(fresh & inner)
-            def _():
-                token_copy(s, c, tok_send.at[s, c], onward).start()
-
-            def pack(q, carry):
-                chosen = pick[pl.ds(pl.multiple_of(q * local, local), local), :]
-                rows = jnp.dot(chosen, tok[s, c], preferred_element_type=f32).astype(bf16)
-                slots[s, q, c] = rows.reshape(experts, CAP, width)
-                return carry
-
-            lax.fori_loop(0, rest, pack, 0)
-            for d in range(rest - 1):
-                away_copy(s, d, c).start()
-            return carry
-
-        return lax.fori_loop(0, CHUNKS, chunk, carry)
+                for c in range(2, CHUNKS + 1):
+                    own_copy(way, c).start()
+
+        return carry
 
     def expert_step(k):
         s = lookup(ORDER, p, k)
@@ -207,7 +227,7 @@
                 away_copy(s, d, c).wait_recv()
 
         def one(e, carry):
-            @pl.when(k == 0)
+            @pl.when(k == 1)
             def _():
                 for copy in weight_copies(e):
                     copy.wait()
@@ -219,17 +239,27 @@
                 rows = pl.ds(c * width, width)
                 gate_val = gate_val + jnp.dot(x, gate[e, rows, :], preferred_element_type=f32)
                 up_val = up_val + jnp.dot(x, up[e, rows, :], preferred_element_type=f32)
-            act = (gate_val * jax.nn.sigmoid(gate_val) * up_val).astype(bf16)
-            for c in range(CHUNKS):
-                out = jnp.dot(act, down[e, :, pl.ds(c * width, width)], preferred_element_type=f32).astype(bf16)
+            act[e] = (gate_val * jax.nn.sigmoid(gate_val) * up_val).astype(bf16)
+            return carry
+
+        lax.fori_loop(0, experts, one, 0)
+
+        def two(c, carry):
+            for e in range(experts):
+                columns = pl.ds(pl.multiple_of(c * width, width), width)
+                out = jnp.dot(act[e], down[e, :, columns], preferred_element_type=f32).astype(bf16)
                 slots[s, r, c, e] = out[:CAP]
                 for d in range(rest - 1):
                     away[s, d, c, e] = out[(d + 1) * CAP : (d + 2) * CAP]
-            for d in range(rest - 1):
-                back_copy(s, d, e).start()
-            return carry
-
-        lax.fori_loop(0, experts, one, 0)
+
+            @pl.when(k > 0)
+            def _():
+                for d in range(rest - 1):
+                    back_copy(s, d, c).start()
+
+            return carry
+
+        lax.fori_loop(0, CHUNKS, two, 0)
 
     def make_mix(s, i):
         def rows(q, carry):
@@ -246,10 +276,9 @@
 
         lax.fori_loop(0, tokens // BLOCK, rows, 0)
 
-    def returns(s):
+    def returned(s, c):
         for d in range(rest - 1):
-            for e in range(experts):
-                back_copy(s, d, e).wait_recv()
+            back_copy(s, d, c).wait_recv()
 
     def combine(s, i, c, here):
         acc = jnp.dot(mix[i, 0, here], slots[s, r, c].reshape(local, width), preferred_element_type=f32)
@@ -265,6 +294,7 @@
         lax.fori_loop(0, tokens // HALF, body, 0)
 
     def send_part(s, i, c, passed):
+        returned(s, c)
         if passed:
             part_arrival(s, c).wait_recv()
             token_copy(s, c, tok_send.at[s, c], below).wait_send()
@@ -278,17 +308,48 @@
         by_rows(step)
         part_copy(s, c).start()
 
+    near = jnp.clip(PLANES - 1 - p, 0, PLANES - 1)
+    end = jnp.where(p == 1, PLANES - 1, 0)
+    far = PLANES - 1 - end
+
     def main_step(k, carry):
         lax.fori_loop(lookup(LOW, p, k), lookup(HIGH, p, k), unpack_step, 0)
-        expert_step(k)
-
-        @pl.when((k > 0) & jnp.logical_not(inner))
+
+        @pl.when(inner & (k == PLANES - 1))
+        def _():
+            make_mix(end, 0)
+            make_mix(far, 1)
+            send_part(end, 0, 0, True)
+            send_part(end, 0, 1, True)
+            send_part(far, 1, 0, True)
+
+        def expert_turn(i, carry):
+            expert_step(jnp.where(i == 0, k, 0))
+            return carry
+
+        own_turn = jnp.where(inner, PLANES - 1, 1)
+        lax.fori_loop(0, jnp.where(k == own_turn, 2, 1), expert_turn, 0)
+
+        @pl.when(k == PLANES - 1)
+        def _():
+            for c in range(CHUNKS):
+                for d in range(rest - 1):
+                    back_copy(p, d, c).start()
+
+        @pl.when(jnp.logical_not(inner))
         def _():
             s = lookup(ORDER, p, k)
-            returns(s)
             make_mix(s, 0)
 
+            @pl.when(k < PLANES - 1)
+            def _():
+                unpack_start(k + 1)
+
             def chunk(c, carry):
+                @pl.when(k < PLANES - 1)
+                def _():
+                    unpack_chunk(k + 1, c)
+
                 send_part(s, 0, c, False)
                 return carry
 
@@ -296,14 +357,18 @@
 
         return carry
 
-    lax.fori_loop(0, PLANES, main_step, 0)
+    unpack_step(0, 0)
+    lax.fori_loop(1, PLANES, main_step, 0)
 
     @pl.when(inner)
     def _():
-        near = PLANES - 1 - p
-        end = jnp.where(p == 1, PLANES - 1, 0)
-        far = PLANES - 1 - end
-        returns(near)
+        def two(c, carry):
+            send_part(end, 0, c, True)
+            send_part(far, 1, c - 1, True)
+            return carry
+
+        lax.fori_loop(2, CHUNKS, two, 0)
+        send_part(far, 1, CHUNKS - 1, True)
         make_mix(near, 0)
 
         def one(c, carry):
@@ -311,50 +376,43 @@
             return carry
 
         lax.fori_loop(0, CHUNKS, one, 0)
-        returns(end)
-        returns(far)
-        make_mix(end, 0)
-        make_mix(far, 1)
-
-        def two(c, carry):
-            send_part(end, 0, c, True)
-            send_part(far, 1, c, True)
-            return carry
-
-        lax.fori_loop(0, CHUNKS, two, 0)
 
     def fin_copy(c):
         return pltpu.make_async_copy(fin.at[c % 2], out_hbm.at[:, pl.ds(c * width, width)], fin_sem.at[c % 2])
 
-    returns(p)
     make_mix(p, 0)
     for c in range(CHUNKS):
         hid_copy = pltpu.make_async_copy(hidden_hbm.at[:, pl.ds(c * width, width)], hid, hid_sem)
         hid_copy.start()
+        returned(p, c)
         hid_copy.wait()
 
-        @pl.when(jnp.logical_not(first))
+        def own(here):
+            hid[here] = hid[here] + combine(p, 0, c, here)
+
+        by_rows(own)
+
+        @pl.when(inner)
         def _():
             part_arrival(p, c).wait_recv()
+            part_arrival(PLANES, c).wait_recv()
 
             def step(here):
-                hid[here] = hid[here] + parts[p, c, here].astype(f32)
+                both = parts[p, c, here].astype(f32) + parts[PLANES, c, here].astype(f32)
+                fin[c % 2, here] = (hid[here] + both).astype(bf16)
 
             by_rows(step)
 
-        @pl.when(jnp.logical_not(last))
-        def _():
-            part_arrival(PLANES, c).wait_recv()
+        @pl.when(jnp.logical_not(inner))
+        def _():
+            index = jnp.where(first, PLANES, p)
+            part_arrival(index, c).wait_recv()
 
             def step(here):
-                hid[here] = hid[here] + parts[PLANES, c, here].astype(f32)
+                fin[c % 2, here] = (hid[here] + parts[index, c, here].astype(f32)).astype(bf16)
 
             by_rows(step)
 
-        def step(here):
-            fin[c % 2, here] = (hid[here] + combine(p, 0, c, here)).astype(bf16)
-
-        by_rows(step)
         fin_copy(c).start()
         if c:
             fin_copy(c - 1).wait()
@@ -372,8 +430,7 @@
         for d in range(rest - 1):
             for c in range(CHUNKS):
                 away_copy(s, d, c).wait_send()
-            for e in range(experts):
-                back_copy(s, d, e).wait_send()
+                back_copy(s, d, c).wait_send()
 
         @pl.when(k > 0)
         def _():
@@ -413,6 +470,7 @@
             pltpu.VMEM(w_down.shape, bf16),
             pltpu.VMEM((rest * experts * CAP, tokens), bf16),
             pltpu.VMEM((2, rest, tokens, experts * CAP), bf16),
+            pltpu.VMEM((experts, rest * CAP, ffe), bf16),
             pltpu.VMEM((tokens, width), f32),
             pltpu.VMEM((2, tokens, width), bf16),
             dma((CHUNKS,)),
@@ -426,8 +484,8 @@
             dma((PLANES,)),
             dma((PLANES, rest - 1, CHUNKS)),
             dma((PLANES, rest - 1, CHUNKS)),
-            dma((PLANES, rest - 1, experts)),
-            dma((PLANES, rest - 1, experts)),
+            dma((PLANES, rest - 1, CHUNKS)),
+            dma((PLANES, rest - 1, CHUNKS)),
             dma((PLANES, CHUNKS)),
             dma((PLANES + 1, CHUNKS)),
             dma,

time: 320 us -> 272 us (0.85)
  Pallas kernels: 272 us -> 227 us
    pallas_call x1, Pallas kernels: 272 us -> 227 us  [experts_and_back(): pl.pallas_call(functools.partial(moe_kernel, rest), in_specs=[anywhere] *...]
where the time goes in v1:
time: 272 us; the launch traced here: 271 us
  Pallas kernels  227 us (83%)
  waiting for transfers between devices  16.3 us (6%)
  other arithmetic  8.53 us (3%)
  starting transfers between devices  7.07 us (3%)
  local copies, waits for them, and re-layouts  5.87 us (2%)
  matrix products  5.75 us (2%)
    pallas_call x1, Pallas kernels, experts_and_back(): pl.pallas_call(functools.partial(moe_kernel, rest), in_specs=[anywhere] *...  227 us
    all_to_all x1, waiting for transfers between devices, per_device(): lax.all_to_all(gated, 'tp', split_axis=0, concat_axis=1, tiled=True)  13.5 us
    dot_general x1, matrix products, per_device(): mixed = jnp.dot(regrouped, proj_weight, preferred_element_type=f32)  5.54 us
  transfers between devices with their start and end apart: 2, of which 2 were waited for; matrix products, arithmetic and copies ran while one was open for 0% of the time, Pallas kernels for 0%

profile of v1, /device:TPU:16, one launch (start us, length us, event | category | flops | bytes accessed | tf_op | source)
XLA Modules:
  0.0 270.5 jit_solution(5952864013568672554)
XLA Ops:
  0.0 0.7 convert_element_type.41
  0.7 0.1 slice.55
  0.8 1.9 convert_multiply_fusion
  2.7 0.1 broadcast_in_dim.54
  2.7 3.4 %collective-permute-start = (f32[2,384]{1,0:T(2,128)S(1)}, f32[2,384]{1,0:T(2,128)S(1)}, u32[]{:S(2)}, u32[]{:S(2)}) collective-permute-start(f32[2,384]{1,0:T(2,128)S(1)} %pad_maximum_fusion.2), channel_id=1, source_target_pairs={{0,4},{4,8},{8,12},{12,16},{16,20},{20,24},{24,28},{1,5},{5,9},{9,... | collective-permute-start | bytes 9224 | tf_op jit(solution)/shard_map/ppermute | solution.py:506
  6.2 0.0 copy-done.2
  6.2 0.0 copy-done.5
  6.2 0.1 pad.3.clone
  6.3 2.8 %collective-permute-done = f32[2,384]{1,0:T(2,128)S(1)} collective-permute-done((f32[2,384]{1,0:T(2,128)S(1)}, f32[2,384]{1,0:T(2,128)S(1)}, u32[]{:S(2)}, u32[]{:S(2)}) %collective-permute-start) | collective-permute-done | bytes 3104 | tf_op jit(solution)/shard_map/ppermute | solution.py:506
  9.1 0.1 fusion.17
  9.2 0.1 fusion.15
  9.3 0.0 copy-done.1
  9.3 3.3 %fusion.6 = bf16[2048,256]{1,0:T(8,128)(2,1)} fusion(f32[2,256]{1,0:T(2,128)S(1)} %slice.59, f32[2048,256]{1,0:T(8,128)S(1)} %convert_multiply_fusion, bf16[2048,256]{1,0:T(8,128)(2,1)S(1)} %copy-done.1, f32[256]{0:T(256)S(1)} %bitcast.19, f32[256]{0:T(256)S(1)} %bitcast.20, f32[256]{0:T(256)S(1)} %bitcast.18, pred[2048]{0:T(1024)(128)(4,1)S(1)} %convert_compare_fusion, ...), kind=kLoop, calls=%fused_computation.11 | loop fusion | flops 6815744 | bytes 4205568 | tf_op jit(solution)/shard_map/convert_element_type | solution.py:556
  12.7 3.6 %all-to-all-start = ((bf16[4,512,256]{2,1,0:T(8,128)(2,1)}), bf16[4,512,256]{2,1,0:T(8,128)(2,1)S(1)}, u32[]{:S(2)}, u32[]{:S(2)}) async-start(bf16[4,512,256]{2,1,0:T(8,128)(2,1)} %bitcast.3), calls=%async_computation | async-start | bytes 2097152 | tf_op jit(solution)/shard_map/all_to_all | solution.py:557
  16.4 0.2 select_reduce_fusion.1
  16.6 0.7 maximum_maximum_fusion.meta_hbm
  17.3 13.5 %all-to-all-done = bf16[4,512,256]{2,1,0:T(8,128)(2,1)S(1)} async-done(((bf16[4,512,256]{2,1,0:T(8,128)(2,1)}), bf16[4,512,256]{2,1,0:T(8,128)(2,1)S(1)}, u32[]{:S(2)}, u32[]{:S(2)}) %all-to-all-start) | async-done | bytes 1048608 | tf_op jit(solution)/shard_map/all_to_all | solution.py:557
  30.7 0.5 copy.15
  31.3 0.0 copy-start.4
  31.3 5.5 %multiply_reduce_fusion = (f32[512]{0:T(512)S(1)}, f32[512,2048]{1,0:T(8,128)S(1)}) fusion(bf16[512,1024]{0,1:T(8,128)(2,1)S(1)} %bitcast.14, bf16[1024,2048]{1,0:T(8,128)(2,1)} %param.19, bf16[512,2048]{1,0:T(8,128)(2,1)} %param.13), kind=kOutput, calls=%fused_computation.1 | convolution fusion | flops 2151677440 | bytes 11536384 | tf_op jit(solution)/shard_map/dot_general | solution.py:559
  36.8 1.9 copy-done
  38.8 1.7 multiply_convert_fusion.normed_hbm
  40.5 226.8 %shard_map.127 = bf16[512,2048]{1,0:T(8,128)(2,1)} custom-call(bf16[512,2048]{1,0:T(8,128)(2,1)} %multiply_convert_fusion.normed_hbm, f32[8,512]{1,0:T(8,128)} %maximum_maximum_fusion.meta_hbm, f32[512,2048]{1,0:T(8,128)} %copy-done, bf16[4,2048,512]{2,1,0:T(8,128)(2,1)} %gate_hbm.1, bf16[4,2048,512]{2,1,0:T(8,128)(2,1)} %up_hbm.1, ...), custom_call_target="tpu_custom_call" | custom-call | flops 12884901888 | bytes 33554432 | tf_op jit(solution)/shard_map/pallas_call | solution.py:456
  267.4 3.2 %copy.17 = bf16[512,2048]{1,0:T(8,128)(2,1)} copy(bf16[512,2048]{1,0:T(8,128)(2,1)} %shard_map.127) | data formatting | bytes 4194304
  (18 shorter events, 0.1 us)
Async XLA Ops:
  0.8 5.4 %copy-start.2 = (s32[2048]{0:T(1024)S(1)}, s32[2048]{0:T(1024)}, u32[]{:S(2)}) copy-start(s32[2048]{0:T(1024)} %param.18) | copy-start | bytes 24580
  0.8 5.4 %copy-start.5 = (bf16[3,256]{1,0:T(4,128)(2,1)S(1)}, bf16[3,256]{1,0:T(4,128)(2,1)}, u32[]{:S(2)}) copy-start(bf16[3,256]{1,0:T(4,128)(2,1)} %param.17) | copy-start | bytes 4612
  0.8 8.5 %copy-start.1 = (bf16[2048,256]{1,0:T(8,128)(2,1)S(1)}, bf16[2048,256]{1,0:T(8,128)(2,1)}, u32[]{:S(2)}) copy-start(bf16[2048,256]{1,0:T(8,128)(2,1)} %param.16) | copy-start | bytes 3145732
  2.7 6.4 %collective-permute-start = (f32[2,384]{1,0:T(2,128)S(1)}, f32[2,384]{1,0:T(2,128)S(1)}, u32[]{:S(2)}, u32[]{:S(2)}) collective-permute-start(f32[2,384]{1,0:T(2,128)S(1)} %pad_maximum_fusion.2), channel_id=1, source_target_pairs={{0,4},{4,8},{8,12},{12,16},{16,20},{20,24},{24,28},{1,5},{5,9},{9,... | collective-permute-start | bytes 9224 | tf_op jit(solution)/shard_map/ppermute | solution.py:506
  12.7 3.7 %copy-start.3 = (s32[512,2]{0,1:T(2,128)S(1)}, s32[512,2]{0,1:T(2,128)}, u32[]{:S(2)}) copy-start(s32[512,2]{0,1:T(2,128)} %param.21) | copy-start | bytes 12292
  12.7 3.9 %copy-start.6 = (f32[512,2]{0,1:T(2,128)S(1)}, f32[512,2]{0,1:T(2,128)}, u32[]{:S(2)}) copy-start(f32[512,2]{0,1:T(2,128)} %param.22) | copy-start | bytes 12292
  12.7 18.1 %all-to-all-start = ((bf16[4,512,256]{2,1,0:T(8,128)(2,1)}), bf16[4,512,256]{2,1,0:T(8,128)(2,1)S(1)}, u32[]{:S(2)}, u32[]{:S(2)}) async-start(bf16[4,512,256]{2,1,0:T(8,128)(2,1)} %bitcast.3), calls=%async_computation | async-start | bytes 2097152 | tf_op jit(solution)/shard_map/all_to_all | solution.py:557
  31.3 7.5 %copy-start.4 = (f32[2048]{0:T(1024)S(1)}, f32[2048]{0:T(1024)}, u32[]{:S(2)}) copy-start(f32[2048]{0:T(1024)} %param.20) | copy-start | bytes 24580
  36.8 1.9 copy-start

commit v2 on v1

--- a/solution.py
+++ b/solution.py
@@ -32,13 +32,22 @@
 
 def moe_kernel(
     rest,
-    normed_hbm,
-    meta_hbm,
-    hidden_hbm,
+    share_weights,
+    share_mix,
+    conv_hbm,
+    entry_hbm,
+    exit_hbm,
+    docs_hbm,
+    taps_hbm,
+    routes_hbm,
+    proj_hbm,
+    residual_hbm,
+    gain_hbm,
     gate_hbm,
     up_hbm,
     down_hbm,
     out_hbm,
+    hidden_hbm,
     tok,
     meta,
     slots,
@@ -53,8 +62,20 @@
     act,
     hid,
     fin,
+    taps,
+    routes,
+    gain,
+    rim_out,
+    rim_in,
+    edge,
     load_sem,
-    meta_load_sem,
+    proj_sem,
+    residual_sem,
+    small_sem,
+    rim_send,
+    rim_recv,
+    deal_send,
+    deal_recv,
     weight_sem,
     own_sem,
     own_meta_sem,
@@ -70,6 +91,7 @@
     part_recv,
     hid_sem,
     fin_sem,
+    *extra,
 ):
     me = lax.axis_index("sp")
     p, r = me // rest, lax.rem(me, rest)
@@ -110,31 +132,171 @@
     def part_arrival(index, c):
         return remote(tok.at[0, c], parts.at[index, c], part_send.at[0, c], part_recv.at[index, c], below)
 
-    loads = [
-        pltpu.make_async_copy(normed_hbm.at[:, pl.ds(c * width, width)], tok.at[p, c], load_sem.at[c]) for c in range(CHUNKS)
-    ]
-    meta_load = pltpu.make_async_copy(meta_hbm, meta.at[p], meta_load_sem)
-
     def weight_copies(e):
         pairs = ((gate_hbm, gate), (up_hbm, up), (down_hbm, down))
         return [pltpu.make_async_copy(a.at[e], b.at[e], weight_sem.at[i, e]) for i, (a, b) in enumerate(pairs)]
 
-    meta_load.start()
-    for load in loads:
+    tp_size = lax.axis_size("tp")
+    t = lax.axis_index("tp")
+    positions, channels = conv_hbm.shape
+    depth = proj_hbm.shape[0]
+    if share_weights:
+        conv_in, entry = up.at[0, :, 0:channels], up.at[0, :, channels : 2 * channels]
+        exit_gate, docs = up.at[1, :, 0:channels], up.at[1, :, channels : channels + 128]
+        proj = [gate.at[c // 2, pl.ds((c % 2) * depth, depth), :] for c in range(CHUNKS)]
+
+        def gated(j):
+            return down.at[j, :, width : width + channels]
+
+    else:
+        conv_s, docs_s, proj_s, gated_s = extra[:4]
+        conv_in, entry, exit_gate, docs = conv_s.at[0], conv_s.at[1], conv_s.at[2], docs_s
+        proj = [proj_s.at[c] for c in range(CHUNKS)]
+
+        def gated(j):
+            return gated_s.at[j]
+
+    def dealt(j):
+        return mix.at[j // rest, lax.rem(j, rest)] if share_mix else extra[-1].at[j]
+
+    def deal_copy(offset):
+        j = lax.rem(t + offset, tp_size)
+        return pltpu.make_async_remote_copy(
+            src_ref=gated(j),
+            dst_ref=dealt(t),
+            send_sem=deal_send.at[offset],
+            recv_sem=deal_recv.at[t],
+            device_id={"tp": j},
+            device_id_type=MESH,
+        )
+
+    def deal_arrival(offset):
+        j = lax.rem(t + tp_size - offset, tp_size)
+        return pltpu.make_async_remote_copy(
+            src_ref=gated(j),
+            dst_ref=dealt(j),
+            send_sem=deal_send.at[offset],
+            recv_sem=deal_recv.at[j],
+            device_id={"tp": j},
+            device_id_type=MESH,
+        )
+
+    sources = ((conv_hbm, conv_in), (entry_hbm, entry), (docs_hbm, docs), (exit_hbm, exit_gate))
+    loads = [pltpu.make_async_copy(a, b, load_sem.at[i]) for i, (a, b) in enumerate(sources)]
+    smalls = [
+        pltpu.make_async_copy(a, b, small_sem.at[i])
+        for i, (a, b) in enumerate(((taps_hbm, taps), (routes_hbm, routes), (gain_hbm, gain)))
+    ]
+    proj_loads = [
+        pltpu.make_async_copy(proj_hbm.at[:, pl.ds(c * width, width)], proj[c], proj_sem.at[c]) for c in range(CHUNKS)
+    ]
+    residual_loads = [
+        pltpu.make_async_copy(residual_hbm.at[:, pl.ds(c * width, width)], tok.at[p, c], residual_sem.at[c])
+        for c in range(CHUNKS)
+    ]
+    for load in loads + smalls + proj_loads + residual_loads:
         load.start()
+
+    devices = PLANES * rest
+    final_device = me == devices - 1
+    behind, ahead = lax.max(me - 1, 0), lax.min(me + 1, devices - 1)
     barrier = pltpu.get_barrier_semaphore()
-
-    @pl.when(jnp.logical_not(first))
-    def _():
-        pl.semaphore_signal(barrier, inc=1, device_id={"sp": below}, device_id_type=MESH)
-
-    @pl.when(jnp.logical_not(last))
-    def _():
-        pl.semaphore_signal(barrier, inc=1, device_id={"sp": above}, device_id_type=MESH)
+    greetings = ((jnp.logical_not(first), below), (jnp.logical_not(last), above), (me > 0, behind), (me < devices - 1, ahead))
+    for there, device in greetings:
+
+        @pl.when(there)
+        def _():
+            pl.semaphore_signal(barrier, inc=1, device_id={"sp": device}, device_id_type=MESH)
 
     for peer in peers:
         pl.semaphore_signal(barrier, inc=1, device_id={"sp": peer}, device_id_type=MESH)
-    pl.semaphore_wait(barrier, rest - 1 + jnp.where(inner, 2, 1))
+    for offset in range(1, tp_size):
+        pl.semaphore_signal(barrier, inc=1, device_id={"tp": lax.rem(t + offset, tp_size)}, device_id_type=MESH)
+    line = jnp.where(inner, 2, 1) + jnp.where((me == 0) | final_device, 1, 2)
+    pl.semaphore_wait(barrier, rest - 1 + tp_size - 1 + line)
+
+    for load in loads[:3]:
+        load.wait()
+    smalls[0].wait()
+    rim = remote(rim_out, rim_in, rim_send, rim_recv, ahead)
+
+    def tail(base):
+        rows = pl.ds(pl.multiple_of(base - 16, 16), 16)
+        return (conv_in[rows, :].astype(f32) * entry[rows, :].astype(f32))[8:], docs[rows, :].astype(f32)[8:]
+
+    rim_values, rim_docs = tail(positions)
+    rim_out[:, :channels] = rim_values
+    rim_out[:, channels:] = rim_docs
+
+    @pl.when(me < devices - 1)
+    def _():
+        rim.start()
+
+    @pl.when(me == 0)
+    def _():
+        rim_in[:, :channels] = jnp.zeros((8, channels), f32)
+        rim_in[:, channels:] = jnp.full((8, 128), -1.0, f32)
+
+    loads[3].wait()
+
+    def conv_block(j, target):
+        @pl.when((j == 0) & (me > 0))
+        def _():
+            rim.wait_recv()
+
+        def piece(b, carry):
+            base = j * tokens + b * BLOCK
+            rows = pl.ds(pl.multiple_of(base, BLOCK), BLOCK)
+            value = conv_in[rows, :].astype(f32) * entry[rows, :].astype(f32)
+            doc = docs[rows, :].astype(f32)
+
+            @pl.when(base == 0)
+            def _():
+                edge[...] = rim_in[...]
+
+            @pl.when(base > 0)
+            def _():
+                edge[:, :channels], edge[:, channels:] = tail(base)
+
+            long = jnp.concatenate([edge[:, :channels], value], axis=0)
+            long_docs = jnp.concatenate([edge[:, channels:], doc], axis=0)
+            total = jnp.zeros((BLOCK, channels), f32)
+            reach = taps.shape[0] - 1
+            for k in range(reach + 1):
+                term = taps[k : k + 1, :].astype(f32) * long[8 - reach + k : 8 - reach + k + BLOCK]
+                if k < reach:
+                    same = jnp.where(long_docs[8 - reach + k : 8 - reach + k + BLOCK] == doc, 1.0, 0.0)
+                    term = term * jnp.concatenate([same] * (channels // 128), axis=1)
+                total = total + term
+            target[pl.ds(pl.multiple_of(b * BLOCK, BLOCK), BLOCK), :] = (
+                exit_gate[rows, :].astype(f32) * total
+            ).astype(bf16)
+            return carry
+
+        lax.fori_loop(0, tokens // BLOCK, piece, 0)
+
+    for offset in sorted(range(1, tp_size), key=lambda o: abs(2 * o - tp_size)):
+        j = lax.rem(t + offset, tp_size)
+        conv_block(j, gated(j))
+        deal_copy(offset).start()
+    conv_block(t, dealt(t))
+
+    smalls[1].wait()
+    names = lax.broadcasted_iota(jnp.int32, (devices * experts, tokens), 0).astype(f32)
+    hits = [jnp.where(names == routes[i : i + 1, :], 1.0, 0.0) for i in range(2)]
+
+    def earlier(q, carry):
+        row = lax.broadcasted_iota(jnp.int32, (BLOCK, tokens), 0) + q * BLOCK
+        column = lax.broadcasted_iota(jnp.int32, (BLOCK, tokens), 1)
+        pick[pl.ds(pl.multiple_of(q * BLOCK, BLOCK), BLOCK), :] = jnp.where(row < column, 1.0, 0.0).astype(bf16)
+        return carry
+
+    lax.fori_loop(0, tokens // BLOCK, earlier, 0)
+    before = jnp.dot((hits[0] + hits[1]).astype(bf16), pick[0:tokens, :], preferred_element_type=f32)
+    for i in range(2):
+        rank = jnp.sum(hits[i] * before, axis=0, keepdims=True)
+        meta[p, i : i + 1, :] = routes[i : i + 1, :] * CAP + rank
+    meta[p, 2:8, :] = routes[2:8, :]
 
     def own_copy(way, c):
         device = (above, below)[way]
@@ -144,15 +306,59 @@
 
     ways = (jnp.logical_not(last), jnp.logical_not(first))
     middle = (p == 1, p == PLANES - 2)
-    meta_load.wait()
-    for c in range(CHUNKS + 1):
-        if c:
-            loads[c - 1].wait()
+
+    def start_own(c):
         for way in range(2):
 
             @pl.when(ways[way] if c < 2 else ways[way] & jnp.logical_not(middle[way]))
             def _():
                 own_copy(way, c).start()
+
+    start_own(0)
+    smalls[2].wait()
+    for load in proj_loads + residual_loads:
+        load.wait()
+    for offset in range(1, tp_size):
+        deal_arrival(offset).wait_recv()
+    blocks = tokens // BLOCK
+
+    def hidden_copy(q):
+        return pltpu.make_async_copy(hid.at[lax.rem(q, 2), 0:CHUNKS], hidden_hbm.at[:, q], hid_sem.at[lax.rem(q, 2)])
+
+    def project(q, carry):
+        rows = pl.ds(pl.multiple_of(q * BLOCK, BLOCK), BLOCK)
+        slot = lax.rem(q, 2)
+
+        @pl.when(q > 1)
+        def _():
+            hidden_copy(q - 2).wait()
+
+        squares = jnp.zeros((BLOCK, 1), f32)
+        for c in range(CHUNKS):
+            acc = tok[p, c, rows].astype(f32)
+            for j in range(tp_size):
+                weights = proj[c][pl.ds(j * channels, channels), :]
+                acc = acc + jnp.dot(dealt(j)[rows, :], weights, preferred_element_type=f32)
+            hid[slot, c] = acc
+            squares = squares + jnp.sum(acc * acc, axis=1, keepdims=True)
+        scale = lax.rsqrt(squares * (1.0 / (CHUNKS * width)) + epsilon)
+        for c in range(CHUNKS):
+            normed = hid[slot, c] * scale * gain[:, c * width : (c + 1) * width]
+            tok[p, c, rows] = normed.astype(bf16)
+        hidden_copy(q).start()
+        return carry
+
+    lax.fori_loop(0, blocks, project, 0)
+    for c in range(1, CHUNKS + 1):
+        start_own(c)
+    for offset in range(1, tp_size):
+        deal_copy(offset).wait_send()
+    for q in range(max(blocks - 2, 0), blocks):
+        hidden_copy(q).wait()
+
+    @pl.when(me < devices - 1)
+    def _():
+        rim.wait_send()
 
     for e in range(experts):
         for copy in weight_copies(e):
@@ -378,19 +584,29 @@
         lax.fori_loop(0, CHUNKS, one, 0)
 
     def fin_copy(c):
-        return pltpu.make_async_copy(fin.at[c % 2], out_hbm.at[:, pl.ds(c * width, width)], fin_sem.at[c % 2])
+        return pltpu.make_async_copy(fin, out_hbm.at[:, pl.ds(c * width, width)], fin_sem)
+
+    def hid_load(c):
+        return pltpu.make_async_copy(hidden_hbm.at[c], hid.at[c % 2, 0:blocks], hid_sem.at[c % 2])
+
+    def piece(c, here):
+        return hid[c % 2, pl.ds(here.start // BLOCK, HALF // BLOCK)].reshape(HALF, width)
 
     make_mix(p, 0)
+    hid_load(0).start()
     for c in range(CHUNKS):
-        hid_copy = pltpu.make_async_copy(hidden_hbm.at[:, pl.ds(c * width, width)], hid, hid_sem)
-        hid_copy.start()
+        hid_load(c).wait()
+        if c + 1 < CHUNKS:
+            hid_load(c + 1).start()
         returned(p, c)
-        hid_copy.wait()
 
         def own(here):
-            hid[here] = hid[here] + combine(p, 0, c, here)
+            total = piece(c, here) + combine(p, 0, c, here)
+            hid[c % 2, pl.ds(here.start // BLOCK, HALF // BLOCK)] = total.reshape(HALF // BLOCK, BLOCK, width)
 
         by_rows(own)
+        if c:
+            fin_copy(c - 1).wait()
 
         @pl.when(inner)
         def _():
@@ -399,7 +615,7 @@
 
             def step(here):
                 both = parts[p, c, here].astype(f32) + parts[PLANES, c, here].astype(f32)
-                fin[c % 2, here] = (hid[here] + both).astype(bf16)
+                fin[here] = (piece(c, here) + both).astype(bf16)
 
             by_rows(step)
 
@@ -409,13 +625,11 @@
             part_arrival(index, c).wait_recv()
 
             def step(here):
-                fin[c % 2, here] = (hid[here] + parts[index, c, here].astype(f32)).astype(bf16)
+                fin[here] = (piece(c, here) + parts[index, c, here].astype(f32)).astype(bf16)
 
             by_rows(step)
 
         fin_copy(c).start()
-        if c:
-            fin_copy(c - 1).wait()
     fin_copy(CHUNKS - 1).wait()
 
     for way in range(2):
@@ -446,21 +660,47 @@
     lax.fori_loop(0, PLANES, drain, 0)
 
 
-def experts_and_back(normed, meta, hidden, w_gate, w_up, w_down):
+def layer(conv_input, input_gate, output_gate, docs, taps, routes, proj, residual, gain, w_gate, w_up, w_down):
     rest = lax.axis_size("sp") // PLANES
+    tp_size = lax.axis_size("tp")
     experts, model, ffe = w_gate.shape
-    tokens = normed.shape[0]
+    tokens = residual.shape[0]
+    positions, channels = conv_input.shape
+    depth = proj.shape[0]
     width = model // CHUNKS
+    pieces = max(CHUNKS, tokens // BLOCK)
     dma = pltpu.SemaphoreType.DMA
     anywhere = pl.BlockSpec(memory_space=pl.ANY)
+    share_weights = (
+        experts >= max(CHUNKS, tp_size)
+        and (model, ffe, ffe) == (positions, width, tokens)
+        and 2 * depth <= model
+        and 2 * channels <= ffe
+        and channels >= 128
+        and width + channels <= model
+    )
+    share_mix = tp_size == 2 * rest and channels == experts * CAP
+    extra = []
+    if not share_weights:
+        extra += [
+            pltpu.VMEM((3, positions, channels), bf16),
+            pltpu.VMEM(docs.shape, bf16),
+            pltpu.VMEM((CHUNKS, depth, width), bf16),
+            pltpu.VMEM((tp_size, tokens, channels), bf16),
+        ]
+    if not share_mix:
+        extra += [pltpu.VMEM((tp_size, tokens, channels), bf16)]
     return pl.pallas_call(
-        functools.partial(moe_kernel, rest),
-        in_specs=[anywhere] * 6,
-        out_specs=anywhere,
-        out_shape=jax.ShapeDtypeStruct((tokens, model), bf16),
+        functools.partial(moe_kernel, rest, share_weights, share_mix),
+        in_specs=[anywhere] * 12,
+        out_specs=[anywhere] * 2,
+        out_shape=[
+            jax.ShapeDtypeStruct((tokens, model), bf16),
+            jax.ShapeDtypeStruct((CHUNKS, tokens // BLOCK, BLOCK, width), f32),
+        ],
         scratch_shapes=[
             pltpu.VMEM((PLANES, CHUNKS, tokens, width), bf16),
-            pltpu.VMEM((PLANES,) + meta.shape, f32),
+            pltpu.VMEM((PLANES,) + routes.shape, f32),
             pltpu.VMEM((PLANES, rest, CHUNKS, experts, CAP, width), bf16),
             pltpu.VMEM((PLANES, rest - 1, CHUNKS, experts, CAP, width), bf16),
             pltpu.VMEM((PLANES, rest - 1, CHUNKS, experts, CAP, width), bf16),
@@ -471,10 +711,22 @@
             pltpu.VMEM((rest * experts * CAP, tokens), bf16),
             pltpu.VMEM((2, rest, tokens, experts * CAP), bf16),
             pltpu.VMEM((experts, rest * CAP, ffe), bf16),
-            pltpu.VMEM((tokens, width), f32),
-            pltpu.VMEM((2, tokens, width), bf16),
+            pltpu.VMEM((2, pieces, BLOCK, width), f32),
+            pltpu.VMEM((tokens, width), bf16),
+            pltpu.VMEM(taps.shape, bf16),
+            pltpu.VMEM(routes.shape, f32),
+            pltpu.VMEM(gain.shape, f32),
+            pltpu.VMEM((8, channels + 128), f32),
+            pltpu.VMEM((8, channels + 128), f32),
+            pltpu.VMEM((8, channels + 128), f32),
+            dma((4,)),
             dma((CHUNKS,)),
+            dma((CHUNKS,)),
+            dma((3,)),
             dma,
+            dma,
+            dma((tp_size,)),
+            dma((tp_size,)),
             dma((3, experts)),
             dma((2, CHUNKS)),
             dma((2,)),
@@ -488,35 +740,17 @@
             dma((PLANES, rest - 1, CHUNKS)),
             dma((PLANES, CHUNKS)),
             dma((PLANES + 1, CHUNKS)),
+            dma((2,)),
             dma,
-            dma((2,)),
-        ],
+        ]
+        + extra,
         compiler_params=pltpu.CompilerParams(collective_id=0, has_side_effects=True, vmem_limit_bytes=67043328),
         cost_estimate=pl.CostEstimate(
             flops=6 * PLANES * rest * experts * CAP * model * ffe,
-            bytes_accessed=2 * (w_gate.size * 3 + 4 * normed.size),
+            bytes_accessed=2 * (w_gate.size * 3 + 4 * residual.size),
             transcendentals=PLANES * rest * experts * CAP * ffe,
         ),
-    )(normed, meta, hidden, w_gate, w_up, w_down)
-
-
-def from_behind(x, axis, by):
-    devices = lax.axis_size(axis)
-    pairs = [(i, i + by) for i in range(devices) if 0 <= i + by < devices]
-    return lax.ppermute(x, axis, pairs)
-
-
-def slot_table(ids, weights, experts):
-    tokens = ids.shape[1]
-    names = jnp.arange(experts, dtype=jnp.int32)[:, None]
-    hits = [ids[j][None, :] == names for j in range(2)]
-    named = (hits[0] | hits[1]).astype(bf16)
-    at = jnp.arange(tokens, dtype=jnp.int32)
-    earlier = (at[:, None] < at[None, :]).astype(bf16)
-    before = jnp.dot(named, earlier, preferred_element_type=f32)
-    rank = [jnp.sum(jnp.where(hits[j], before, 0.0), axis=0) for j in range(2)]
-    slot = [ids[j].astype(f32) * CAP + rank[j] for j in range(2)]
-    return jnp.concatenate([jnp.stack(slot), weights, jnp.zeros((4, tokens), f32)], axis=0)
+    )(conv_input, input_gate, output_gate, docs, taps, routes, proj, residual, gain, w_gate, w_up, w_down)[0]
 
 
 def per_device(
@@ -534,33 +768,13 @@
     w_up,
     w_down,
 ):
-    kernel_width = conv_taps.shape[0]
-    rim_rows = kernel_width - 1
-    meta = slot_table(expert_ids.T, expert_weight.T, w_gate.shape[0] * lax.axis_size("sp"))
-
-    product = input_gate.astype(f32) * conv_input.astype(f32)
-    doc_float = doc_ids.astype(f32)
-    doc_rim = jnp.broadcast_to(doc_float[-rim_rows:, None], (rim_rows, 128))
-    rim = from_behind(jnp.concatenate([product[-rim_rows:], doc_rim], axis=1), "sp", 1)
-    channels = product.shape[1]
-    prev_in, prev_ids = rim[:, :channels], rim[:, channels]
-    prev_ids = jnp.where(lax.axis_index("sp") == 0, -1.0, prev_ids)
-    padded_in = jnp.concatenate([prev_in, product], axis=0)
-    padded_ids = jnp.concatenate([prev_ids, doc_float], axis=0)
-    length = product.shape[0]
-    conv_sum = jnp.zeros(product.shape, f32)
-    for offset in range(kernel_width):
-        same_doc = padded_ids[offset : offset + length] == doc_float
-        term = conv_taps[offset].astype(f32)[None, :] * padded_in[offset : offset + length]
-        conv_sum = conv_sum + jnp.where(same_doc[:, None], term, 0.0)
-    gated = (output_gate.astype(f32) * conv_sum).astype(bf16)
-    regrouped = lax.all_to_all(gated, "tp", split_axis=0, concat_axis=1, tiled=True)
-
-    mixed = jnp.dot(regrouped, proj_weight, preferred_element_type=f32)
-    hidden = residual_in.astype(f32) + mixed
-    scale_rows = lax.rsqrt(jnp.mean(hidden * hidden, axis=-1, keepdims=True) + epsilon)
-    normed = (hidden * scale_rows * norm_gain[None, :]).astype(bf16)
-    return experts_and_back(normed, meta, hidden, w_gate, w_up, w_down)
+    tokens = expert_ids.shape[0]
+    routes = jnp.concatenate([expert_ids.T.astype(f32), expert_weight.T, jnp.zeros((4, tokens), f32)], axis=0)
+    docs = jnp.broadcast_to(doc_ids.astype(bf16)[:, None], (doc_ids.shape[0], 128))
+    gain = norm_gain[None, :]
+    return layer(
+        conv_input, input_gate, output_gate, docs, conv_taps, routes, proj_weight, residual_in, gain, w_gate, w_up, w_down
+    )
 
 
 def solution(mesh):

time: 272 us -> 258 us (0.949)
  Pallas kernels: 227 us -> 251 us
  waiting for transfers between devices: 16.3 us -> 0 us
  starting transfers between devices: 7.07 us -> 0 us
  other arithmetic: 8.53 us -> 2.74 us
  matrix products: 5.75 us -> 0 us
    pallas_call x1, Pallas kernels: 227 us -> 251 us  [layer(): pl.pallas_call(functools.partial(moe_kernel, rest, share_weights, share_m...]
    all_to_all x1 -> x0, waiting for transfers between devices: 13.5 us -> none  [per_device(): lax.all_to_all(gated, 'tp', split_axis=0, concat_axis=1, tiled=True)]
    dot_general x2 -> x0, matrix products: 5.75 us -> none  [the longest x1 5.54 us: per_device(): mixed = jnp.dot(regrouped, proj_weight, preferred_element_type=f32)]
    convert_element_type x3 -> x2, other arithmetic: 5.77 us -> 1.39 us  [the longest x1 0.7 us: per_device(): doc_ids.astype(bf16)[:, None]]
    all_to_all x1 -> x0, starting transfers between devices: 3.65 us -> none  [per_device(): lax.all_to_all(gated, 'tp', split_axis=0, concat_axis=1, tiled=True)]
    ppermute x1 -> x0, starting transfers between devices: 3.42 us -> none  [from_behind(): return lax.ppermute(x, axis, pairs)]
    ppermute x1 -> x0, waiting for transfers between devices: 2.81 us -> none  [from_behind(): return lax.ppermute(x, axis, pairs)]
  transfers between devices with their start and end apart: 2 -> 0, of which waited for: 2 -> 0; matrix products, arithmetic and copies ran while one was open for 0% -> 0% of each run, Pallas kernels for 0% -> 0%
where the time goes in v2:
time: 258 us
  Pallas kernels  251 us (97%)
  local copies, waits for them, and re-layouts  4.37 us (2%)
  other arithmetic  2.74 us (1%)
    pallas_call x1, Pallas kernels, layer(): pl.pallas_call(functools.partial(moe_kernel, rest, share_weights, share_m...  251 us

profile of v2, /device:TPU:16, one launch (start us, length us, event | category | flops | bytes accessed | tf_op | source)
XLA Modules:
  0.0 258.1 jit_solution(14531731353357927391)
XLA Ops:
  0.0 0.1 pad.2.clone
  0.1 0.7 convert_element_type.9
  0.8 0.7 convert_bitcast_fusion
  1.5 1.4 maximum_maximum_fusion.routes_hbm
  2.8 1.1 broadcast_in_dim.12.docs_hbm
  4.0 250.9 %shard_map.127 = (bf16[512,2048]{1,0:T(8,128)(2,1)}, f32[4,4,128,512]{3,2,1,0:T(8,128)}) custom-call(bf16[2048,256]{1,0:T(8,128)(2,1)} %conv_hbm.1, bf16[2048,256]{1,0:T(8,128)(2,1)} %entry_hbm.1, bf16[2048,256]{1,0:T(8,128)(2,1)} %exit_hbm.1, bf16[2048,128]{1,0:T(8,128)(2,1)} %broadcast_in_dim.12.docs_hbm, bf16[3,256]{1,0:T(4,128)(2,1)} %taps_hbm.1, ...), custom_call_target="tpu_custom_call" | custom-call | flops 12884901888 | bytes 33554432 | tf_op jit(solution)/shard_map/pallas_call | solution.py:693
  254.9 3.2 %copy.15 = bf16[512,2048]{1,0:T(8,128)(2,1)} copy(bf16[512,2048]{1,0:T(8,128)(2,1)} %get-tuple-element.6) | data formatting | bytes 4194304
  (1 shorter events, 0.0 us)
